TPU v7x, 32 devices: a whole 2x2x4 slice. The times are simulated.
32 devices in a mesh: ep: 8 (over z, x), tp: 4 (over y, core).
Axes of the slice: x: 2, y: 2, z: 4, core: 2. Of those that a mesh axis runs over, the one named last changes fastest.
Arguments:
- tokens: bfloat16 [192, 2048], P('ep'), may hold values from -12 to 12
- state: float32 [192, 16, 128, 256], P('ep', 'tp'), may hold values from -6 to 6
- w_query: bfloat16 [2048, 2048], P(None, 'tp'), may hold values from -0.125 to 0.125
- w_key: bfloat16 [2048, 2048], P(None, 'tp'), may hold values from -0.125 to 0.125
- w_value: bfloat16 [2048, 4096], P(None, 'tp'), may hold values from -0.125 to 0.125
- w_outgate: bfloat16 [2048, 4096], P(None, 'tp'), may hold values from -0.125 to 0.125
- decay_down: bfloat16 [2048, 16], replicated, may hold values from -0.125 to 0.125
- decay_up: bfloat16 [16, 2048], P(None, 'tp'), may hold values from -9 to 9
- decay_bias: float32 [2048], P('tp'), may hold values from -6 to 4
- head_gain: float32 [256], replicated, may hold values from 0.1 to 1.9
- w_output: bfloat16 [4096, 2048], P('tp'), may hold values from -0.09375 to 0.09375
- norm1_gain: float32 [2048], P('tp'), may hold values from 0.1 to 1.9
- route_ids: int32 [192, 6], P('ep'), may hold values from 0 to 31, all different within a row; in each aligned block of 24 rows (0 to 23, 24 to 47, ...) at most 5 rows name the same one
- route_weight: float32 [192, 6], P('ep'), may hold values from 0.1 to 1
- exp_gate: bfloat16 [32, 2048, 512], P('ep', 'tp'), may hold values from -0.125 to 0.125
- exp_up: bfloat16 [32, 2048, 512], P('ep', 'tp'), may hold values from -0.125 to 0.125
- exp_down: bfloat16 [32, 512, 2048], P('ep', None, 'tp'), may hold values from -0.25 to 0.25
- sh_gate: bfloat16 [2048, 512], P('tp'), may hold values from -0.125 to 0.125
- sh_up: bfloat16 [2048, 512], P('tp'), may hold values from -0.125 to 0.125
- sh_down: bfloat16 [512, 2048], P(None, 'tp'), may hold values from -0.25 to 0.25
- norm2_gain: float32 [2048], P('tp'), may hold values from 0.1 to 1.9
Outputs:
- layer_out: bfloat16 [192, 2048], P('ep', 'tp')
Inputs may be any that keep to these rules, and one draw needn't show every extreme that they name: `route_ids`: each row names 6 different experts. Among the rows of one index of ep (aligned blocks of 24 rows) no expert is named by more than 5 rows, and in some blocks one expert is named by exactly 5.
All inputs are finite; a program needn't handle non-finite values.
Results may differ from a plain program's by a relative error of at most 0.02.
Values may be sent and summed in bfloat16 or wider, within the bound.
A program may use at most 64 MiB of HBM per device.

v0:
```python
import jax
import jax.numpy as jnp
from jax import lax
from jax.sharding import PartitionSpec as P

res_scale = 2.0**0.5
decay_tau = 16.0
norm_eps = 1e-05


def settle(values):
    return lax.optimization_barrier(values.astype(jnp.bfloat16)).astype(jnp.float32)


def project(left, right):
    return jnp.dot(left, right, preferred_element_type=jnp.float32)


def apply_norm(values, sums, squares, width, gain):
    mean_val = sums[:, None] / width
    spread = squares[:, None] / width - mean_val * mean_val
    return (values - mean_val) * lax.rsqrt(spread + norm_eps) * gain


def per_device(
    tokens,
    state,
    w_query,
    w_key,
    w_value,
    w_outgate,
    decay_down,
    decay_up,
    decay_bias,
    head_gain,
    w_output,
    norm1_gain,
    route_ids,
    route_weight,
    exp_gate,
    exp_up,
    exp_down,
    sh_gate,
    sh_up,
    sh_down,
    norm2_gain,
):
    row_count, width = tokens.shape
    head_count, key_dim, val_dim = (state.shape[1], state.shape[2], state.shape[3])
    tp_count = lax.axis_size("tp")
    ep_count = lax.axis_size("ep")
    col_count = width // tp_count
    col_start = lax.axis_index("tp") * col_count
    queries = settle(project(tokens, w_query)).reshape(
        row_count, head_count, key_dim
    ) * key_dim ** (-0.5)
    key_rows = settle(project(tokens, w_key)).reshape(row_count, head_count, key_dim)
    values = settle(project(tokens, w_value)).reshape(row_count, head_count, val_dim)
    gate_pre = settle(project(tokens, w_outgate)).reshape(row_count, head_count, val_dim)
    decay_low = lax.optimization_barrier(project(tokens, decay_down).astype(jnp.bfloat16))
    log_decay = (jax.nn.log_sigmoid(project(decay_low, decay_up) + decay_bias) / decay_tau).reshape(
        row_count, head_count, key_dim
    )
    carried = jnp.einsum(
        "bhk,bhkv->bhv", queries * jnp.exp(log_decay), state, precision=lax.Precision.HIGHEST
    )
    attended = carried + jnp.sum(queries * key_rows, -1, keepdims=True) * values
    inv_norm = lax.rsqrt(jnp.mean(attended * attended, -1, keepdims=True) + norm_eps)
    head_out = (
        (attended * inv_norm * head_gain * jax.nn.silu(gate_pre))
        .astype(jnp.bfloat16)
        .reshape(row_count, head_count * val_dim)
    )
    partial_out = project(head_out, w_output)
    mixed = settle(
        lax.psum_scatter(
            partial_out.astype(jnp.bfloat16), "tp", scatter_dimension=1, tiled=True
        ).astype(jnp.float32)
    )
    own_tokens = lax.dynamic_slice_in_dim(tokens, col_start, col_count, 1).astype(jnp.float32)
    own_resid = res_scale * own_tokens + mixed
    first_sums, first_squares = lax.psum(
        (jnp.sum(own_resid, -1), jnp.sum(own_resid * own_resid, -1)), "tp"
    )
    normed_mid = apply_norm(own_resid, first_sums, first_squares, width, norm1_gain)
    normed_mid = lax.optimization_barrier(normed_mid.astype(jnp.bfloat16))
    top_count = route_ids.shape[1]
    local_count = exp_gate.shape[0]
    expert_count = local_count * ep_count
    capacity = max(2, row_count * top_count // expert_count + 1)
    flat_ids = route_ids.reshape(row_count * top_count)
    onehot = (flat_ids[:, None] == jnp.arange(expert_count, dtype=jnp.int32)[None, :]).astype(
        jnp.int32
    )
    ranks = jnp.sum((jnp.cumsum(onehot, 0) - 1) * onehot, 1)
    slots = flat_ids * capacity + ranks
    placement = (
        slots[:, None] == jnp.arange(expert_count * capacity, dtype=jnp.int32)[None, :]
    ).astype(jnp.bfloat16)
    pair_rows = jnp.repeat(normed_mid, top_count, axis=0)
    outgoing = jnp.einsum(
        "ps,pc->sc", placement, pair_rows, preferred_element_type=jnp.float32
    ).astype(jnp.bfloat16)
    outgoing = outgoing.reshape(ep_count, local_count, capacity, col_count)
    incoming = lax.all_to_all(outgoing, "ep", split_axis=0, concat_axis=0, tiled=True)
    gate_part = jnp.einsum("secd,edf->secf", incoming, exp_gate, preferred_element_type=jnp.float32)
    up_part = jnp.einsum("secd,edf->secf", incoming, exp_up, preferred_element_type=jnp.float32)
    shared_gate_part = project(normed_mid, sh_gate)
    shared_up_part = project(normed_mid, sh_up)
    gate_sum, up_sum, shared_gate_sum, shared_up_sum = (
        lax.psum(gate_part.astype(jnp.bfloat16), "tp").astype(jnp.float32),
        lax.psum(up_part.astype(jnp.bfloat16), "tp").astype(jnp.float32),
        lax.psum(shared_gate_part.astype(jnp.bfloat16), "tp").astype(jnp.float32),
        lax.psum(shared_up_part.astype(jnp.bfloat16), "tp").astype(jnp.float32),
    )
    inner = (jax.nn.silu(settle(gate_sum)) * settle(up_sum)).astype(jnp.bfloat16)
    shared_inner = (jax.nn.silu(settle(shared_gate_sum)) * settle(shared_up_sum)).astype(
        jnp.bfloat16
    )
    expert_out = jnp.einsum(
        "secf,efd->secd", inner, exp_down, preferred_element_type=jnp.float32
    ).astype(jnp.bfloat16)
    returned = lax.all_to_all(expert_out, "ep", split_axis=0, concat_axis=0, tiled=True)
    picked = jnp.einsum(
        "ps,sc->pc",
        placement,
        returned.reshape(expert_count * capacity, col_count),
        preferred_element_type=jnp.float32,
    )
    routed = jnp.sum(picked.reshape(row_count, top_count, col_count) * route_weight[:, :, None], 1)
    mixture = routed + project(shared_inner, sh_down)
    out_resid = res_scale * normed_mid.astype(jnp.float32) + mixture
    last_sums, last_squares = lax.psum(
        (jnp.sum(out_resid, -1), jnp.sum(out_resid * out_resid, -1)), "tp"
    )
    return apply_norm(out_resid, last_sums, last_squares, width, norm2_gain).astype(jnp.bfloat16)


def solution(mesh):
    in_specs = (
        P("ep", None),
        P("ep", "tp", None, None),
        P(None, "tp"),
        P(None, "tp"),
        P(None, "tp"),
        P(None, "tp"),
        P(),
        P(None, "tp"),
        P("tp"),
        P(),
        P("tp", None),
        P("tp"),
        P("ep", None),
        P("ep", None),
        P("ep", "tp", None),
        P("ep", "tp", None),
        P("ep", None, "tp"),
        P("tp", None),
        P("tp", None),
        P(None, "tp"),
        P("tp"),
    )
    out_specs = P("ep", "tp")
    return jax.shard_map(
        per_device, mesh=mesh, in_specs=in_specs, out_specs=out_specs, check_vma=False
    )
```

profile of v0, /device:TPU:0, one launch (start us, length us, event | category | flops | bytes accessed | tf_op | source)
XLA Modules:
  0.0 142.7 jit_solution(752916315707150363)
XLA Ops:
  6.5 0.0 reduce-scatter.2.cloned.1.call-start
  6.6 2.2 %convolution_convert_fusion.5 = bf16[24,512]{1,0:T(8,128)(2,1)S(1)} fusion(bf16[24,2048]{1,0:T(8,128)(2,1)} %param.21, bf16[2048,512]{1,0:T(8,128)(2,1)} %param.23), kind=kOutput, calls=%fused_computation.23 | convolution fusion | flops 50343936 | bytes 2220032 | tf_op jit(solution)/shard_map/dot_general | solution.py:16
  8.8 0.2 convolution_convert_fusion.8
  8.9 0.2 fusion.49
  9.2 2.0 %convolution_convert_fusion.4 = bf16[24,512]{1,0:T(8,128)(2,1)S(1)} fusion(bf16[24,2048]{1,0:T(8,128)(2,1)S(1)} %copy-done.1, bf16[2048,512]{1,0:T(8,128)(2,1)} %param.24), kind=kOutput, calls=%fused_computation.22 | convolution fusion | flops 50343936 | bytes 2220032 | tf_op jit(solution)/shard_map/dot_general | solution.py:16
  11.2 2.8 %convolution_convert_fusion.3 = bf16[24,1024]{1,0:T(8,128)(2,1)S(1)} fusion(bf16[24,2048]{1,0:T(8,128)(2,1)S(1)} %copy-done.1, bf16[2048,1024]{1,0:T(8,128)(2,1)} %param.25), kind=kOutput, calls=%fused_computation.17 | convolution fusion | flops 100687872 | bytes 4341760 | tf_op jit(solution)/shard_map/dot_general | solution.py:16
  14.1 0.1 reshape.119
  14.1 8.6 %fusion.59 = f32[24,4,1,256]{3,2,1,0:T(1,128)S(1)} fusion(f32[24,4,128,1]{2,3,1,0:T(1,128)S(1)} %bitcast.80, f32[24,4,128,256]{3,2,1,0:T(8,128)} %param.22), kind=kOutput, calls=%fused_computation.88 | convolution fusion | flops 37748736 | bytes 12730368 | tf_op jit(solution)/shard_map/bhk,bhkv->bhv/dot_general | solution.py:64
  22.7 0.1 reduce_sum.74
  22.8 0.2 multiply_reduce_fusion
  23.0 2.8 %convolution_convert_fusion.2 = bf16[24,1024]{1,0:T(8,128)(2,1)S(1)} fusion(bf16[24,2048]{1,0:T(8,128)(2,1)S(1)} %copy-done.1, bf16[2048,1024]{1,0:T(8,128)(2,1)} %param.26), kind=kOutput, calls=%fused_computation.16 | convolution fusion | flops 100687872 | bytes 4341760 | tf_op jit(solution)/shard_map/dot_general | solution.py:16
  25.9 0.1 reshape.121
  25.9 0.1 fusion.39
  26.1 3.5 %convolution_convert_fusion = bf16[24,2048]{1,0:T(8,128)(2,1)} fusion(bf16[24,1024]{1,0:T(8,128)(2,1)S(1)} %bitcast.81, bf16[1024,2048]{1,0:T(8,128)(2,1)} %param.31), kind=kOutput, calls=%fused_computation | convolution fusion | flops 100712448 | bytes 4341760 | tf_op jit(solution)/shard_map/dot_general | solution.py:16
  29.6 0.0 reduce-scatter.2.cloned.1.call-update
  29.6 0.1 copy.48
  29.7 0.1 eq.57
  29.9 0.6 reduce-window.6
  30.4 0.2 slice_reduce_fusion
  30.7 0.1 bitcast_bitcast_fusion
  30.8 21.4 %reduce-scatter.2.cloned.1.call-done = bf16[24,512]{1,0:T(8,128)(2,1)} async-done(((bf16[24,2048]{1,0:T(8,128)(2,1)}), bf16[24,512]{1,0:T(8,128)(2,1)}) %reduce-scatter.2.cloned.1.call-update) | async-done | bytes 24592 | tf_op jit(solution)/shard_map/reduce_scatter | solution.py:76
  52.2 0.9 fusion.51
  53.0 5.8 %all-reduce.2 = (f32[24]{0:T(128)S(1)}, f32[24]{0:T(128)S(1)}) all-reduce(f32[24]{0:T(128)S(1)} %get-tuple-element.6, f32[24]{0:T(128)S(1)} %get-tuple-element.5), channel_id=1, replica_groups=mesh['ep'=8,'tp'=4] {'tp'}, use_global_device_ids=true, to_apply=%region_6.7 | all-reduce | flops 48 | bytes 384 | tf_op jit(solution)/shard_map/psum | solution.py:82
  58.8 0.8 multiply_convert_fusion.1
  59.7 0.1 reshape.115
  59.7 0.3 convolution_convert_fusion.1
  60.0 0.1 reshape.116
  60.1 0.7 copy.52
  60.9 5.7 %all-to-all-start = ((bf16[8,4,5,512]{3,1,2,0:T(4,128)(2,1)}), bf16[8,4,5,512]{3,1,2,0:T(4,128)(2,1)S(1)}, u32[]{:S(2)}, u32[]{:S(2)}) async-start(bf16[8,4,5,512]{3,1,2,0:T(4,128)(2,1)} %copy.52), calls=%async_computation.1 | async-start | bytes 327680 | tf_op jit(solution)/shard_map/all_to_all | solution.py:105
  66.5 0.0 all-reduce.7.cloned.1.call-start
  66.6 0.1 reduce_sum.79
  66.7 0.1 copy.51
  66.7 7.3 %all-to-all-done = bf16[8,4,5,512]{3,1,2,0:T(4,128)(2,1)S(1)} async-done(((bf16[8,4,5,512]{3,1,2,0:T(4,128)(2,1)}), bf16[8,4,5,512]{3,1,2,0:T(4,128)(2,1)S(1)}, u32[]{:S(2)}, u32[]{:S(2)}) %all-to-all-start) | async-done | bytes 163872 | tf_op jit(solution)/shard_map/all_to_all | solution.py:105
  74.1 1.1 fusion.19
  75.2 0.6 copy-done.2
  75.8 1.1 fusion.22
  76.9 29.9 %all-reduce.7.cloned.1.call-done = (bf16[8,4,5,512]{3,0,2,1:T(8,128)(2,1)}, bf16[8,4,5,512]{3,0,2,1:T(8,128)(2,1)}) async-done(((bf16[8,4,5,512]{3,0,2,1:T(8,128)(2,1)}, bf16[8,4,5,512]{3,0,2,1:T(8,128)(2,1)}), (bf16[8,4,5,512]{3,0,2,1:T(8,128)(2,1)}, bf16[8,4,5,512]{3,0,2,1:T(8,128)(2,1)})) %all-reduce.7.cloned.1.call-update) | async-done | bytes 327696 | tf_op jit(solution)/shard_map/psum | solution.py:112
  106.8 2.2 %fusion.16 = bf16[8,4,5,512]{3,0,2,1:T(8,128)(2,1)S(1)} fusion(bf16[4,512,512]{2,1,0:T(8,128)(2,1)} %param.37, bf16[8,4,5,512]{3,0,2,1:T(8,128)(2,1)} %get-tuple-element.15, bf16[8,4,5,512]{3,0,2,1:T(8,128)(2,1)} %get-tuple-element.16), kind=kOutput, calls=%fused_computation.13 | convolution fusion | flops 84623360 | bytes 2588672 | tf_op jit(solution)/shard_map/secf,efd->secd/dot_general | solution.py:120
  109.0 0.7 copy.55
  109.7 5.5 %all-to-all-start.1 = ((bf16[8,4,5,512]{3,1,2,0:T(4,128)(2,1)}), bf16[8,4,5,512]{3,1,2,0:T(4,128)(2,1)S(1)}, u32[]{:S(2)}, u32[]{:S(2)}) async-start(bf16[8,4,5,512]{3,1,2,0:T(4,128)(2,1)} %copy.55), calls=%async_computation.2 | async-start | bytes 327680 | tf_op jit(solution)/shard_map/all_to_all | solution.py:123
  115.2 0.2 convolution_convert_fusion.6
  115.4 1.2 convolution_convert_fusion.7
  116.7 10.9 %all-reduce.3 = (bf16[24,512]{1,0:T(8,128)(2,1)S(1)}, bf16[24,512]{1,0:T(8,128)(2,1)S(1)}) all-reduce(bf16[24,512]{1,0:T(8,128)(2,1)S(1)} %convolution_convert_fusion.6, bf16[24,512]{1,0:T(8,128)(2,1)S(1)} %convolution_convert_fusion.7), channel_id=1, replica_groups=mesh['ep'=8,'tp'=4] {'tp'}, use_global_device_ids=true, to_apply=%region_14.15 | all-reduce | flops 24576 | bytes 98304 | tf_op jit(solution)/shard_map/psum | solution.py:114
  127.6 0.1 reshape.128
  127.7 0.2 fusion.15
  127.9 1.3 fusion.58
  129.3 5.9 %all-reduce.1 = (f32[24]{0:T(128)S(1)}, f32[24]{0:T(128)S(1)}) all-reduce(f32[24]{0:T(128)S(1)} %get-tuple-element.8, f32[24]{0:T(128)S(1)} %get-tuple-element.7), channel_id=1, replica_groups=mesh['ep'=8,'tp'=4] {'tp'}, use_global_device_ids=true, to_apply=%region_18.19 | all-reduce | flops 48 | bytes 384 | tf_op jit(solution)/shard_map/psum | solution.py:133
  135.2 0.7 multiply_convert_fusion
  (41 shorter events, 0.4 us)
Async XLA Ops:
  6.5 67.6 %copy-start = (bf16[4,512,512]{2,1,0:T(8,128)(2,1)S(1)}, bf16[4,512,512]{2,1,0:T(8,128)(2,1)}, u32[]{:S(2)}) copy-start(bf16[4,512,512]{2,1,0:T(8,128)(2,1)} %param.36) | copy-start | bytes 6291460
  6.5 2.2 %copy-start.1 = (bf16[24,2048]{1,0:T(8,128)(2,1)S(1)}, bf16[24,2048]{1,0:T(8,128)(2,1)}, u32[]{:S(2)}) copy-start(bf16[24,2048]{1,0:T(8,128)(2,1)} %param.21) | copy-start | bytes 294916
  6.5 2.2 %copy-start.4 = (bf16[2048,16]{0,1:T(8,128)(2,1)S(1)}, bf16[2048,16]{0,1:T(8,128)(2,1)}, u32[]{:S(2)}) copy-start(bf16[2048,16]{0,1:T(8,128)(2,1)} %param.27) | copy-start | bytes 196612
  6.5 2.4 %copy-start.9 = (bf16[16,512]{1,0:T(8,128)(2,1)S(1)}, bf16[16,512]{1,0:T(8,128)(2,1)}, u32[]{:S(2)}) copy-start(bf16[16,512]{1,0:T(8,128)(2,1)} %param.28) | copy-start | bytes 49156
  6.5 2.4 %copy-start.11 = (f32[512]{0:T(512)S(1)}, f32[512]{0:T(512)}, u32[]{:S(2)}) copy-start(f32[512]{0:T(512)} %param.29) | copy-start | bytes 6148
  6.5 45.6 %reduce-scatter.2.cloned.1.call-start = ((), (), s32[]{:S(2)}) async-start(), calls=%async_computation.3 | async-start | bytes 122880 | tf_op jit(solution)/shard_map/reduce_scatter | solution.py:76
  23.0 2.9 %copy-start.8 = (f32[256]{0:T(256)S(1)}, f32[256]{0:T(256)}, u32[]{:S(2)}) copy-start(f32[256]{0:T(256)} %param.30) | copy-start | bytes 3076
  26.1 3.5 %copy-start.5 = (s32[24,6]{0,1:T(8,128)S(1)}, s32[24,6]{0,1:T(8,128)}, u32[]{:S(2)}) copy-start(s32[24,6]{0,1:T(8,128)} %param.33) | copy-start | bytes 1732
  26.1 32.7 %copy-start.6 = (f32[512]{0:T(512)S(1)}, f32[512]{0:T(512)}, u32[]{:S(2)}) copy-start(f32[512]{0:T(512)} %param.32) | copy-start | bytes 6148
  60.9 13.2 %all-to-all-start = ((bf16[8,4,5,512]{3,1,2,0:T(4,128)(2,1)}), bf16[8,4,5,512]{3,1,2,0:T(4,128)(2,1)S(1)}, u32[]{:S(2)}, u32[]{:S(2)}) async-start(bf16[8,4,5,512]{3,1,2,0:T(4,128)(2,1)} %copy.52), calls=%async_computation.1 | async-start | bytes 327680 | tf_op jit(solution)/shard_map/all_to_all | solution.py:105
  66.5 40.2 %all-reduce.7.cloned.1.call-start = ((), (), s32[]{:S(2)}) async-start(), calls=%async_computation.4 | async-start | bytes 655360 | tf_op jit(solution)/shard_map/psum | solution.py:112
  74.1 1.7 %copy-start.2 = (bf16[4,512,512]{2,1,0:T(8,128)(2,1)S(1)}, bf16[4,512,512]{2,1,0:T(8,128)(2,1)}, u32[]{:S(2)}) copy-start(bf16[4,512,512]{2,1,0:T(8,128)(2,1)} %param.35) | copy-start | bytes 6291460
  76.8 38.4 %copy-start.3 = (bf16[512,512]{1,0:T(8,128)(2,1)S(1)}, bf16[512,512]{1,0:T(8,128)(2,1)}, u32[]{:S(2)}) copy-start(bf16[512,512]{1,0:T(8,128)(2,1)} %param.39) | copy-start | bytes 1572868
  106.8 20.9 %copy-start.10 = (f32[24,6]{0,1:T(8,128)S(1)}, f32[24,6]{0,1:T(8,128)}, u32[]{:S(2)}) copy-start(f32[24,6]{0,1:T(8,128)} %param.34) | copy-start | bytes 1732
  109.0 26.2 %copy-start.7 = (f32[512]{0:T(512)S(1)}, f32[512]{0:T(512)}, u32[]{:S(2)}) copy-start(f32[512]{0:T(512)} %param.41) | copy-start | bytes 6148
  109.7 17.8 %all-to-all-start.1 = ((bf16[8,4,5,512]{3,1,2,0:T(4,128)(2,1)}), bf16[8,4,5,512]{3,1,2,0:T(4,128)(2,1)S(1)}, u32[]{:S(2)}, u32[]{:S(2)}) async-start(bf16[8,4,5,512]{3,1,2,0:T(4,128)(2,1)} %copy.55), calls=%async_computation.2 | async-start | bytes 327680 | tf_op jit(solution)/shard_map/all_to_all | solution.py:123
Sparse Core Ops, SparseCore 0:
  29.7 22.3 reduce-scatter.1
  77.0 29.7 all-reduce.6
where the time goes:
time: 143 us
  waiting for transfers between devices  58.6 us (41%)
  matrix products  29.9 us (21%)
  blocking collectives  22.5 us (16%)
  between operations  13.7 us (10%)
  starting transfers between devices  11.3 us (8%)
  other arithmetic  3.59 us (3%)
  local copies, waits for them, and re-layouts  3.1 us (2%)
    psum x1, waiting for transfers between devices, per_device(): lax.psum(up_part.astype(jnp.bfloat16), 'tp').astype(jnp.float32)  29.9 us
    reduce_scatter x1, waiting for transfers between devices, per_device(): lax.psum_scatter(partial_out.astype(jnp.bfloat16), 'tp', scatter_dimensio...  21.4 us
    dot_general x10, matrix products, project(): return jnp.dot(left, right, preferred_element_type=jnp.float32)  16.4 us
    psum x1, blocking collectives, per_device(): lax.psum(shared_up_part.astype(jnp.bfloat16), 'tp').astype(jnp.float32)  10.9 us
    dot_general x1, matrix products, per_device(): jnp.einsum('bhk,bhkv->bhv', queries * jnp.exp(log_decay), state, precisio...  8.56 us
    all_to_all x1, waiting for transfers between devices, per_device(): lax.all_to_all(outgoing, 'ep', split_axis=0, concat_axis=0, tiled=True)  7.35 us
    psum x1, blocking collectives, per_device(): lax.psum((jnp.sum(out_resid, -1), jnp.sum(out_resid * out_resid, -1)), 'tp')  5.88 us
    psum x1, blocking collectives, per_device(): lax.psum((jnp.sum(own_resid, -1), jnp.sum(own_resid * own_resid, -1)), 'tp')  5.76 us
  transfers between devices with their start and end apart: 4, of which 3 were waited for; matrix products, arithmetic and copies ran while one was open for 2% of the time, Pallas kernels for 0%

commit v1 on v0

--- a/solution.py
+++ b/solution.py
@@ -6,6 +6,12 @@
 res_scale = 2.0**0.5
 decay_tau = 16.0
 norm_eps = 1e-05
+
+
+def add_all(shard, axis):
+    pieces = lax.all_gather(shard, axis, axis=0, tiled=False)
+    total = pieces.sum(axis=0)
+    return total
 
 
 def settle(values):
@@ -109,7 +115,7 @@
     shared_up_part = project(normed_mid, sh_up)
     gate_sum, up_sum, shared_gate_sum, shared_up_sum = (
         lax.psum(gate_part.astype(jnp.bfloat16), "tp").astype(jnp.float32),
-        lax.psum(up_part.astype(jnp.bfloat16), "tp").astype(jnp.float32),
+        add_all(up_part.astype(jnp.bfloat16), "tp").astype(jnp.float32),
         lax.psum(shared_gate_part.astype(jnp.bfloat16), "tp").astype(jnp.float32),
         lax.psum(shared_up_part.astype(jnp.bfloat16), "tp").astype(jnp.float32),
     )

time: 143 us -> 150 us (1.049)
  blocking collectives: 22.5 us -> 29.7 us
    all_gather x0 -> x1, blocking collectives: none -> 7.2 us  [add_all(): pieces = lax.all_gather(shard, axis, axis=0, tiled=False)]
  transfers between devices with their start and end apart: 4 -> 4, of which waited for: 3 -> 3; matrix products, arithmetic and copies ran while one was open for 2% -> 3% of each run, Pallas kernels for 0% -> 0%
where the time goes in v1:
time: 150 us
  waiting for transfers between devices  58.6 us (39%)
  matrix products  30.2 us (20%)
  blocking collectives  29.7 us (20%)
  between operations  13.7 us (9%)
  starting transfers between devices  11.3 us (8%)
  other arithmetic  3.68 us (2%)
  local copies, waits for them, and re-layouts  2.52 us (2%)
    psum x1, waiting for transfers between devices, per_device(): lax.psum(gate_part.astype(jnp.bfloat16), 'tp').astype(jnp.float32)  29.9 us
    reduce_scatter x1, waiting for transfers between devices, per_device(): lax.psum_scatter(partial_out.astype(jnp.bfloat16), 'tp', scatter_dimensio...  21.4 us
    dot_general x10, matrix products, project(): return jnp.dot(left, right, preferred_element_type=jnp.float32)  17.5 us
    psum x1, blocking collectives, per_device(): lax.psum(shared_up_part.astype(jnp.bfloat16), 'tp').astype(jnp.float32)  10.9 us
    dot_general x1, matrix products, per_device(): jnp.einsum('bhk,bhkv->bhv', queries * jnp.exp(log_decay), state, precisio...  8.56 us
    all_to_all x1, waiting for transfers between devices, per_device(): lax.all_to_all(outgoing, 'ep', split_axis=0, concat_axis=0, tiled=True)  7.34 us
    all_gather x1, blocking collectives, add_all(): pieces = lax.all_gather(shard, axis, axis=0, tiled=False)  7.2 us
    psum x1, blocking collectives, per_device(): lax.psum((jnp.sum(out_resid, -1), jnp.sum(out_resid * out_resid, -1)), 'tp')  5.87 us
  transfers between devices with their start and end apart: 4, of which 3 were waited for; matrix products, arithmetic and copies ran while one was open for 3% of the time, Pallas kernels for 0%

profile of v1, /device:TPU:0, one launch (start us, length us, event | category | flops | bytes accessed | tf_op | source)
XLA Modules:
  0.0 149.6 jit_solution(17431064973758879756)
XLA Ops:
  6.5 0.0 reduce-scatter.2.cloned.1.call-start
  6.6 2.2 %convolution_convert_fusion.5 = bf16[24,512]{1,0:T(8,128)(2,1)S(1)} fusion(bf16[24,2048]{1,0:T(8,128)(2,1)} %param.21, bf16[2048,512]{1,0:T(8,128)(2,1)} %param.23), kind=kOutput, calls=%fused_computation.23 | convolution fusion | flops 50343936 | bytes 2220032 | tf_op jit(solution)/shard_map/dot_general | solution.py:22
  8.8 0.2 convolution_convert_fusion.8
  8.9 0.2 fusion.49
  9.2 2.0 %convolution_convert_fusion.4 = bf16[24,512]{1,0:T(8,128)(2,1)S(1)} fusion(bf16[24,2048]{1,0:T(8,128)(2,1)S(1)} %copy-done.1, bf16[2048,512]{1,0:T(8,128)(2,1)} %param.24), kind=kOutput, calls=%fused_computation.22 | convolution fusion | flops 50343936 | bytes 2220032 | tf_op jit(solution)/shard_map/dot_general | solution.py:22
  11.2 2.8 %convolution_convert_fusion.3 = bf16[24,1024]{1,0:T(8,128)(2,1)S(1)} fusion(bf16[24,2048]{1,0:T(8,128)(2,1)S(1)} %copy-done.1, bf16[2048,1024]{1,0:T(8,128)(2,1)} %param.25), kind=kOutput, calls=%fused_computation.17 | convolution fusion | flops 100687872 | bytes 4341760 | tf_op jit(solution)/shard_map/dot_general | solution.py:22
  14.1 0.1 reshape.119
  14.1 8.6 %fusion.59 = f32[24,4,1,256]{3,2,1,0:T(1,128)S(1)} fusion(f32[24,4,128,1]{2,3,1,0:T(1,128)S(1)} %bitcast.82, f32[24,4,128,256]{3,2,1,0:T(8,128)} %param.22), kind=kOutput, calls=%fused_computation.89 | convolution fusion | flops 37748736 | bytes 12730368 | tf_op jit(solution)/shard_map/bhk,bhkv->bhv/dot_general | solution.py:70
  22.7 0.1 reduce_sum.86
  22.8 0.2 multiply_reduce_fusion
  23.0 2.8 %convolution_convert_fusion.2 = bf16[24,1024]{1,0:T(8,128)(2,1)S(1)} fusion(bf16[24,2048]{1,0:T(8,128)(2,1)S(1)} %copy-done.1, bf16[2048,1024]{1,0:T(8,128)(2,1)} %param.26), kind=kOutput, calls=%fused_computation.16 | convolution fusion | flops 100687872 | bytes 4341760 | tf_op jit(solution)/shard_map/dot_general | solution.py:22
  25.9 0.1 reshape.121
  25.9 0.1 fusion.39
  26.1 3.5 %convolution_convert_fusion = bf16[24,2048]{1,0:T(8,128)(2,1)} fusion(bf16[24,1024]{1,0:T(8,128)(2,1)S(1)} %bitcast.83, bf16[1024,2048]{1,0:T(8,128)(2,1)} %param.31), kind=kOutput, calls=%fused_computation | convolution fusion | flops 100712448 | bytes 4341760 | tf_op jit(solution)/shard_map/dot_general | solution.py:22
  29.6 0.1 copy.48
  29.7 0.1 eq.57
  29.9 0.6 reduce-window.6
  30.4 0.2 slice_reduce_fusion
  30.7 0.1 bitcast_bitcast_fusion
  30.8 21.4 %reduce-scatter.2.cloned.1.call-done = bf16[24,512]{1,0:T(8,128)(2,1)} async-done(((bf16[24,2048]{1,0:T(8,128)(2,1)}), bf16[24,512]{1,0:T(8,128)(2,1)}) %reduce-scatter.2.cloned.1.call-update) | async-done | bytes 24592 | tf_op jit(solution)/shard_map/reduce_scatter | solution.py:82
  52.2 0.9 fusion.51
  53.0 5.8 %all-reduce.2 = (f32[24]{0:T(128)S(1)}, f32[24]{0:T(128)S(1)}) all-reduce(f32[24]{0:T(128)S(1)} %get-tuple-element.6, f32[24]{0:T(128)S(1)} %get-tuple-element.5), channel_id=1, replica_groups=mesh['ep'=8,'tp'=4] {'tp'}, use_global_device_ids=true, to_apply=%region_6.7 | all-reduce | flops 48 | bytes 384 | tf_op jit(solution)/shard_map/psum | solution.py:88
  58.8 0.8 multiply_convert_fusion.1
  59.7 0.1 reshape.115
  59.7 0.3 convolution_convert_fusion.1
  60.0 0.1 reshape.116
  60.1 0.7 copy.52
  60.9 5.7 %all-to-all-start = ((bf16[8,4,5,512]{3,1,2,0:T(4,128)(2,1)}), bf16[8,4,5,512]{3,1,2,0:T(4,128)(2,1)S(1)}, u32[]{:S(2)}, u32[]{:S(2)}) async-start(bf16[8,4,5,512]{3,1,2,0:T(4,128)(2,1)} %copy.52), calls=%async_computation.1 | async-start | bytes 327680 | tf_op jit(solution)/shard_map/all_to_all | solution.py:111
  66.5 0.0 all-reduce.6.cloned.1.call-start
  66.6 0.1 reduce_sum.91
  66.7 0.1 copy.51
  66.8 7.3 %all-to-all-done = bf16[8,4,5,512]{3,1,2,0:T(4,128)(2,1)S(1)} async-done(((bf16[8,4,5,512]{3,1,2,0:T(4,128)(2,1)}), bf16[8,4,5,512]{3,1,2,0:T(4,128)(2,1)S(1)}, u32[]{:S(2)}, u32[]{:S(2)}) %all-to-all-start) | async-done | bytes 163872 | tf_op jit(solution)/shard_map/all_to_all | solution.py:111
  74.1 0.4 fusion.19
  74.5 7.2 %all-gather = bf16[32,4,5,512]{3,0,2,1:T(8,128)(2,1)S(1)} all-gather(bf16[8,4,5,512]{3,0,2,1:T(8,128)(2,1)S(1)} %fusion.19), channel_id=2, replica_groups=mesh['ep'=8,'tp'=4] {'tp'}, dimensions={0}, use_global_device_ids=true | all-gather | bytes 819200 | tf_op jit(solution)/shard_map/all_gather | solution.py:12
  81.7 1.1 fusion.22
  82.8 0.1 bitcast_reduce_fusion
  82.9 29.9 %all-reduce.6.cloned.1.call-done = bf16[8,4,5,512]{3,0,2,1:T(8,128)(2,1)} async-done(((bf16[8,4,5,512]{3,0,2,1:T(8,128)(2,1)}), bf16[8,4,5,512]{3,0,2,1:T(8,128)(2,1)}) %all-reduce.6.cloned.1.call-update) | async-done | bytes 163856 | tf_op jit(solution)/shard_map/psum | solution.py:117
  112.8 2.1 %fusion.16 = bf16[8,4,5,512]{3,0,2,1:T(8,128)(2,1)S(1)} fusion(bf16[4,512,512]{2,1,0:T(8,128)(2,1)} %param.37, bf16[8,4,5,512]{3,0,2,1:T(8,128)(2,1)S(1)} %bitcast_reduce_fusion, bf16[8,4,5,512]{3,0,2,1:T(8,128)(2,1)} %all-reduce.6.cloned.1.call-done), kind=kOutput, calls=%fused_computation.13 | convolution fusion | flops 84623360 | bytes 2588672 | tf_op jit(solution)/shard_map/secf,efd->secd/dot_general | solution.py:126
  114.9 0.7 copy.55
  115.6 5.5 %all-to-all-start.1 = ((bf16[8,4,5,512]{3,1,2,0:T(4,128)(2,1)}), bf16[8,4,5,512]{3,1,2,0:T(4,128)(2,1)S(1)}, u32[]{:S(2)}, u32[]{:S(2)}) async-start(bf16[8,4,5,512]{3,1,2,0:T(4,128)(2,1)} %copy.55), calls=%async_computation.2 | async-start | bytes 327680 | tf_op jit(solution)/shard_map/all_to_all | solution.py:129
  121.2 1.2 convolution_convert_fusion.6
  122.4 1.2 convolution_convert_fusion.7
  123.6 10.9 %all-reduce.3 = (bf16[24,512]{1,0:T(8,128)(2,1)S(1)}, bf16[24,512]{1,0:T(8,128)(2,1)S(1)}) all-reduce(bf16[24,512]{1,0:T(8,128)(2,1)S(1)} %convolution_convert_fusion.6, bf16[24,512]{1,0:T(8,128)(2,1)S(1)} %convolution_convert_fusion.7), channel_id=1, replica_groups=mesh['ep'=8,'tp'=4] {'tp'}, use_global_device_ids=true, to_apply=%region_14.15 | all-reduce | flops 24576 | bytes 98304 | tf_op jit(solution)/shard_map/psum | solution.py:120
  134.5 0.1 reshape.129
  134.6 0.2 fusion.15
  134.9 1.3 fusion.58
  136.2 5.9 %all-reduce.1 = (f32[24]{0:T(128)S(1)}, f32[24]{0:T(128)S(1)}) all-reduce(f32[24]{0:T(128)S(1)} %get-tuple-element.8, f32[24]{0:T(128)S(1)} %get-tuple-element.7), channel_id=1, replica_groups=mesh['ep'=8,'tp'=4] {'tp'}, use_global_device_ids=true, to_apply=%region_18.19 | all-reduce | flops 48 | bytes 384 | tf_op jit(solution)/shard_map/psum | solution.py:139
  142.1 0.7 multiply_convert_fusion
  (41 shorter events, 0.4 us)
Async XLA Ops:
  6.5 67.6 %copy-start = (bf16[4,512,512]{2,1,0:T(8,128)(2,1)S(1)}, bf16[4,512,512]{2,1,0:T(8,128)(2,1)}, u32[]{:S(2)}) copy-start(bf16[4,512,512]{2,1,0:T(8,128)(2,1)} %param.36) | copy-start | bytes 6291460
  6.5 2.2 %copy-start.1 = (bf16[24,2048]{1,0:T(8,128)(2,1)S(1)}, bf16[24,2048]{1,0:T(8,128)(2,1)}, u32[]{:S(2)}) copy-start(bf16[24,2048]{1,0:T(8,128)(2,1)} %param.21) | copy-start | bytes 294916
  6.5 2.2 %copy-start.3 = (bf16[2048,16]{0,1:T(8,128)(2,1)S(1)}, bf16[2048,16]{0,1:T(8,128)(2,1)}, u32[]{:S(2)}) copy-start(bf16[2048,16]{0,1:T(8,128)(2,1)} %param.27) | copy-start | bytes 196612
  6.5 2.4 %copy-start.8 = (bf16[16,512]{1,0:T(8,128)(2,1)S(1)}, bf16[16,512]{1,0:T(8,128)(2,1)}, u32[]{:S(2)}) copy-start(bf16[16,512]{1,0:T(8,128)(2,1)} %param.28) | copy-start | bytes 49156
  6.5 2.4 %copy-start.10 = (f32[512]{0:T(512)S(1)}, f32[512]{0:T(512)}, u32[]{:S(2)}) copy-start(f32[512]{0:T(512)} %param.29) | copy-start | bytes 6148
  6.5 45.6 %reduce-scatter.2.cloned.1.call-start = ((), (), s32[]{:S(2)}) async-start(), calls=%async_computation.3 | async-start | bytes 122880 | tf_op jit(solution)/shard_map/reduce_scatter | solution.py:82
  23.0 2.9 %copy-start.7 = (f32[256]{0:T(256)S(1)}, f32[256]{0:T(256)}, u32[]{:S(2)}) copy-start(f32[256]{0:T(256)} %param.30) | copy-start | bytes 3076
  26.1 3.5 %copy-start.4 = (s32[24,6]{0,1:T(8,128)S(1)}, s32[24,6]{0,1:T(8,128)}, u32[]{:S(2)}) copy-start(s32[24,6]{0,1:T(8,128)} %param.33) | copy-start | bytes 1732
  26.1 32.7 %copy-start.5 = (f32[512]{0:T(512)S(1)}, f32[512]{0:T(512)}, u32[]{:S(2)}) copy-start(f32[512]{0:T(512)} %param.32) | copy-start | bytes 6148
  60.9 13.2 %all-to-all-start = ((bf16[8,4,5,512]{3,1,2,0:T(4,128)(2,1)}), bf16[8,4,5,512]{3,1,2,0:T(4,128)(2,1)S(1)}, u32[]{:S(2)}, u32[]{:S(2)}) async-start(bf16[8,4,5,512]{3,1,2,0:T(4,128)(2,1)} %copy.52), calls=%async_computation.1 | async-start | bytes 327680 | tf_op jit(solution)/shard_map/all_to_all | solution.py:111
  66.5 46.2 %all-reduce.6.cloned.1.call-start = ((), (), s32[]{:S(2)}) async-start(), calls=%async_computation.4 | async-start | bytes 327680 | tf_op jit(solution)/shard_map/psum | solution.py:117
  74.1 7.6 %copy-start.2 = (bf16[4,512,512]{2,1,0:T(8,128)(2,1)S(1)}, bf16[4,512,512]{2,1,0:T(8,128)(2,1)}, u32[]{:S(2)}) copy-start(bf16[4,512,512]{2,1,0:T(8,128)(2,1)} %param.35) | copy-start | bytes 6291460
  82.9 51.7 %copy-start.9 = (f32[24,6]{0,1:T(8,128)S(1)}, f32[24,6]{0,1:T(8,128)}, u32[]{:S(2)}) copy-start(f32[24,6]{0,1:T(8,128)} %param.34) | copy-start | bytes 1732
  114.9 27.2 %copy-start.6 = (f32[512]{0:T(512)S(1)}, f32[512]{0:T(512)}, u32[]{:S(2)}) copy-start(f32[512]{0:T(512)} %param.41) | copy-start | bytes 6148
  115.6 18.8 %all-to-all-start.1 = ((bf16[8,4,5,512]{3,1,2,0:T(4,128)(2,1)}), bf16[8,4,5,512]{3,1,2,0:T(4,128)(2,1)S(1)}, u32[]{:S(2)}, u32[]{:S(2)}) async-start(bf16[8,4,5,512]{3,1,2,0:T(4,128)(2,1)} %copy.55), calls=%async_computation.2 | async-start | bytes 327680 | tf_op jit(solution)/shard_map/all_to_all | solution.py:129
Sparse Core Ops, SparseCore 0:
  29.7 22.3 reduce-scatter.1
  82.9 29.8 all-reduce.5
